TPU v7x, 256 devices: a 4x2x16 block of a 4x16x16 slice. The times are simulated.
256 devices in a mesh: grp: 2 (over y), ep: 64 (over z, x), tp: 2 (over core).
Axes of the slice: x: 4, y: 2, z: 16, core: 2. Of those that a mesh axis runs over, the one named last changes fastest.
The devices are a block of a 4x16x16 slice.
Arguments:
- tokens: bfloat16 [32768, 2048], P(('grp', 'ep'), 'tp'), parts along dimension 0, may hold values from -6 to 6
- norm_gain: bfloat16 [2048], P('tp'), may hold values from 0.099609375 to 1.8984375
- w_gate: bfloat16 [64, 2048, 1024], P('ep', None, 'tp'), may hold values from -0.125 to 0.125
- w_up: bfloat16 [64, 2048, 1024], P('ep', None, 'tp'), may hold values from -0.125 to 0.125
- w_down: bfloat16 [64, 1024, 2048], P('ep', 'tp'), may hold values from -0.1875 to 0.1875
- expert_ids: int32 [32768, 2], P(('grp', 'ep')), parts along dimension 0, may hold values from 0 to 63, as said below
- combine: float32 [32768, 2], P(('grp', 'ep')), parts along dimension 0, may hold values from 0.1 to 1
- final_gain: bfloat16 [2048], P('tp'), may hold values from 0.099609375 to 1.8984375
Outputs:
- result: bfloat16 [32768, 2048], P(('grp', 'ep'), 'tp'), parts along dimension 0
There are 2 independent parts, one for each index of `grp`. A program takes and returns all parts, laid end to end along the dimension named above; an argument that names none is the same for every part. Nothing has to cross between parts.
Inputs may be any that keep to these rules, and one draw needn't show every extreme that they name: `expert_ids`: the experts form 4 groups of consecutive ids of equal size; the 2 experts of a row are different and lie in one group. Among the rows of one index of ep no expert is named more than 20 times, and in each such block some expert is named exactly 20 times.
All inputs are finite; a program needn't handle non-finite values.
Results may differ from a plain program's by a relative error of at most 0.0077.
Values may be sent and summed in bfloat16 or wider, within the bound.
A program may use at most 64 MiB of HBM per device.

v0:
```python
import jax
import jax.numpy as jnp
from jax import lax
from jax.sharding import PartitionSpec as P

GROUPS = 4


def total_of_pieces(x, axis):
    parts = lax.all_gather(x, axis)
    return parts.sum(axis=0)


def split_up(x, dim, count):
    lengths = x.shape
    parts = x.reshape(*lengths[:dim], count, lengths[dim] // count, *lengths[dim + 1 :])
    return jnp.moveaxis(parts, dim, 0)


def sent_and_summed(x, axis, dim):
    parts = split_up(x, dim, lax.axis_size(axis))
    arrived = lax.all_to_all(parts, axis, split_axis=0, concat_axis=0, tiled=True)
    return arrived.astype(jnp.float32).sum(axis=0)


def body(tokens, norm_gain, w_gate, w_up, w_down, expert_ids, combine, final_gain):
    eps = 1e-06
    tok_dev, half = tokens.shape
    n_ep = lax.axis_size("ep")
    n_tp = lax.axis_size("tp")
    width = half * n_tp
    exp_dev = w_gate.shape[0]
    experts = exp_dev * n_ep
    per_group = experts // GROUPS
    capacity = tok_dev // 8 * 5 * 2 // per_group
    top = expert_ids.shape[1]
    narrow = tokens.astype(jnp.float32)
    squares = total_of_pieces(jnp.sum(narrow * narrow, axis=1), "tp")
    scale = lax.rsqrt(squares[:, None] / width + eps)
    normed = (narrow * scale * norm_gain.astype(jnp.float32)).astype(jnp.bfloat16)
    columns = normed.shape[1]
    flat = expert_ids.reshape(-1)
    onehot = (flat[:, None] == jnp.arange(experts, dtype=jnp.int32)[None, :]).astype(jnp.int32)
    ranking = jnp.sum(jnp.cumsum(onehot, axis=0) * onehot, axis=1) - 1
    target = flat * capacity + ranking
    sources = jnp.arange(tok_dev * top, dtype=jnp.int32) // top
    owner = jnp.full((experts * capacity,), tok_dev, jnp.int32).at[target].set(sources)
    padded = jnp.concatenate([normed, jnp.zeros((1, columns), jnp.bfloat16)], axis=0)
    outgoing = padded[owner].reshape(n_ep, exp_dev * capacity, columns)
    arrived = lax.all_to_all(outgoing, "ep", split_axis=0, concat_axis=0, tiled=True)
    rows = (
        arrived.reshape(n_ep, exp_dev, capacity, columns)
        .transpose(1, 0, 2, 3)
        .reshape(exp_dev, n_ep * capacity, columns)
    )
    piece = lax.all_gather(rows, "tp", axis=2, tiled=True)
    gate = jnp.einsum("erd,edf->erf", piece, w_gate, preferred_element_type=jnp.float32)
    upper = jnp.einsum("erd,edf->erf", piece, w_up, preferred_element_type=jnp.float32)
    hidden = (jax.nn.silu(gate) * upper).astype(jnp.bfloat16)
    partial_out = jnp.einsum(
        "erf,efd->erd", hidden, w_down, preferred_element_type=jnp.float32
    ).astype(jnp.bfloat16)
    shares = sent_and_summed(partial_out, "tp", 2).astype(jnp.bfloat16)
    homeward = (
        shares.reshape(exp_dev, n_ep, capacity, half)
        .transpose(1, 0, 2, 3)
        .reshape(n_ep, exp_dev * capacity, half)
    )
    returned = lax.all_to_all(homeward, "ep", split_axis=0, concat_axis=0, tiled=True).reshape(
        experts * capacity, half
    )
    picked = returned[target].astype(jnp.float32).reshape(tok_dev, top, half)
    mixed = jnp.sum(picked * combine[:, :, None], axis=1)
    totals = total_of_pieces(jnp.sum(mixed * mixed, axis=1), "tp")
    norm = lax.rsqrt(totals[:, None] / width + eps)
    return (mixed * norm * final_gain.astype(jnp.float32)).astype(jnp.bfloat16)


def solution(mesh):
    placed = (
        P(("grp", "ep"), "tp"),
        P("tp"),
        P("ep", None, "tp"),
        P("ep", None, "tp"),
        P("ep", "tp", None),
        P(("grp", "ep"), None),
        P(("grp", "ep"), None),
        P("tp"),
    )
    return jax.shard_map(
        body, mesh=mesh, in_specs=placed, out_specs=P(("grp", "ep"), "tp"), check_vma=False
    )
```

profile of v0, /device:TPU:33, one launch (start us, length us, event | category | flops | bytes accessed | tf_op | source)
XLA Modules:
  0.0 464.1 jit_solution(18118570353789319803)
XLA Ops:
  6.5 0.0 copy-start
  6.6 0.0 all-gather.6.cloned.1.call-start
  6.6 1.0 copy.16
  7.5 0.1 eq.29
  7.7 0.1 eq.25
  7.8 0.7 broadcast_multiply_fusion
  8.5 1.2 reduce-window.6
  9.7 0.2 slice_reduce_fusion
  10.0 0.1 fusion.21
  10.1 0.1 copy.15
  10.3 0.1 mul.81
  10.4 2.5 scatter_custom_fusion
  12.9 1.2 fusion.17
  14.1 21.9 %all-gather.2 = f32[2,1,256]{2,1,0:T(1,128)S(1)} all-gather(f32[1,1,256]{2,1,0:T(1,128)S(1)} %bitcast.48), channel_id=2, replica_groups=mesh['grp'=2,'ep'=64,'tp'=2] {'tp'}, dimensions={0}, use_global_device_ids=true | all-gather | bytes 3072 | tf_op jit(solution)/shard_map/all_gather | solution.py:10
  36.1 0.7 convert_element_type.38
  36.8 1.2 fusion.19
  38.1 5.1 %gather_fusion = bf16[1280,1024]{1,0:T(8,128)(2,1)} fusion(bf16[257,1024]{1,0:T(8,128)(2,1)S(1)} %concatenate.3, s32[2048]{0:T(1024)S(1)} %pad_clamp_fusion), kind=kCustom, calls=%fused_computation | custom fusion | bytes 5248000 | tf_op jit(solution)/shard_map/gather | solution.py:49
  43.1 5.2 %reshape.113 = bf16[64,20,1024]{2,1,0:T(8,128)(2,1)} reshape(bf16[1280,1024]{1,0:T(8,128)(2,1)} %gather_fusion) | data formatting | bytes 5242880 | tf_op jit(solution)/shard_map/reshape | solution.py:49
  48.3 149.8 %all_to_all.15 = bf16[64,20,1024]{2,1,0:T(8,128)(2,1)} all-to-all(bf16[64,20,1024]{2,1,0:T(8,128)(2,1)} %reshape.113), channel_id=1, replica_groups=mesh['grp'=2,'ep'=64,'tp'=2] {'ep'}, dimensions={0} | all-to-all | bytes 5242880 | tf_op jit(solution)/shard_map/all_to_all | solution.py:50
  198.1 5.2 %reshape_transpose_reshape.6 = bf16[1,1280,1024]{2,1,0:T(8,128)(2,1)} reshape(bf16[64,20,1024]{2,1,0:T(8,128)(2,1)} %all_to_all.15) | data formatting | bytes 5242880 | tf_op jit(solution)/shard_map/reshape;transpose;reshape | solution.py:54
  203.3 0.1 all-gather.6.cloned.1.call-update
  203.3 21.7 %all-gather.6.cloned.1.call-done = bf16[1,1280,2048]{2,1,0:T(8,128)(2,1)} async-done(((bf16[1,1280,1024]{2,1,0:T(8,128)(2,1)}), bf16[1,1280,2048]{2,1,0:T(8,128)(2,1)}) %all-gather.6.cloned.1.call-update) | async-done | bytes 5242896 | tf_op jit(solution)/shard_map/all_gather | solution.py:56
  225.0 7.6 %fusion.2 = f32[1280,512]{1,0:T(8,128)} fusion(bf16[1,1280,2048]{2,1,0:T(8,128)(2,1)} %all-gather.6.cloned.1.call-done, bf16[1,2048,512]{2,1,0:T(8,128)(2,1)} %param.10), kind=kOutput, calls=%fused_computation.6 | convolution fusion | flops 2684354560 | bytes 9961472 | tf_op jit(solution)/shard_map/erd,edf->erf/dot_general | solution.py:57
  232.6 0.0 copy-done
  232.6 10.3 %convolution_convert_fusion = bf16[1280,2048]{1,0:T(8,128)(2,1)} fusion(bf16[1,512,2048]{2,1,0:T(8,128)(2,1)S(1)} %copy-done, bf16[1,1280,2048]{2,1,0:T(8,128)(2,1)} %all-gather.6.cloned.1.call-done, f32[1280,512]{1,0:T(8,128)} %fusion.2, bf16[1,2048,512]{2,1,0:T(8,128)(2,1)} %param.11), kind=kOutput, calls=%fused_computation.3 | convolution fusion | flops 5375262720 | bytes 17301504 | tf_op jit(solution)/shard_map/erf,efd->erd/dot_general | solution.py:60
  242.9 9.5 %reshape.118 = bf16[1,1280,2,1024]{3,2,1,0:T(2,128)(2,1)} reshape(bf16[1280,2048]{1,0:T(8,128)(2,1)} %convolution_convert_fusion) | data formatting | bytes 10485760 | tf_op jit(solution)/shard_map/reshape | solution.py:16
  252.4 4.1 copy.24
  256.5 9.0 %all_to_all.16 = bf16[2,1,1280,1024]{3,2,1,0:T(8,128)(2,1)} all-to-all(bf16[2,1,1280,1024]{3,2,1,0:T(8,128)(2,1)S(1)} %bitcast.44), channel_id=1, replica_groups=mesh['grp'=2,'ep'=64,'tp'=2] {'tp'}, dimensions={0} | all-to-all | bytes 10485760 | tf_op jit(solution)/shard_map/all_to_all | solution.py:22
  265.5 6.2 %reduce_sum.69 = bf16[1280,1024]{1,0:T(8,128)(2,1)} reduce(bf16[2,1,1280,1024]{3,2,1,0:T(8,128)(2,1)} %all_to_all.16, bf16[]{:T(256)} %constant.38.clone.1), dimensions={0,1}, to_apply=%region_6.7 | reduce | flops 1310720 | bytes 7864322 | tf_op jit(solution)/shard_map/reduce_sum | solution.py:23
  271.7 5.1 %reshape_transpose_reshape.7 = bf16[64,20,1024]{2,1,0:T(8,128)(2,1)} reshape(bf16[1280,1024]{1,0:T(8,128)(2,1)} %reduce_sum.69) | data formatting | bytes 5242880 | tf_op jit(solution)/shard_map/reshape;transpose;reshape | solution.py:67
  276.9 0.0 copy-start.1
  276.9 0.0 copy-start.2
  276.9 16.3 %all-to-all-start.2 = ((bf16[64,20,1024]{2,1,0:T(8,128)(2,1)}), bf16[64,20,1024]{2,1,0:T(8,128)(2,1)}, u32[]{:S(2)}, u32[]{:S(2)}) async-start(bf16[64,20,1024]{2,1,0:T(8,128)(2,1)} %reshape_transpose_reshape.7), calls=%async_computation.2 | async-start | bytes 6291456 | tf_op jit(solution)/shard_map/all_to_all | solution.py:69
  293.2 0.0 copy-done.1
  293.2 0.1 copy.20
  293.3 0.0 copy-done.2
  293.4 138.9 %all-to-all-done.2 = bf16[64,20,1024]{2,1,0:T(8,128)(2,1)} async-done(((bf16[64,20,1024]{2,1,0:T(8,128)(2,1)}), bf16[64,20,1024]{2,1,0:T(8,128)(2,1)}, u32[]{:S(2)}, u32[]{:S(2)}) %all-to-all-start.2) | async-done | bytes 2621472 | tf_op jit(solution)/shard_map/all_to_all | solution.py:69
  432.3 5.2 %reshape.119 = bf16[1280,1024]{1,0:T(8,128)(2,1)} reshape(bf16[64,20,1024]{2,1,0:T(8,128)(2,1)} %all-to-all-done.2) | data formatting | bytes 5242880 | tf_op jit(solution)/shard_map/reshape | solution.py:69
  437.4 4.8 %gather_fusion.1 = bf16[512,1024]{1,0:T(8,128)(2,1)S(1)} fusion(bf16[1280,1024]{1,0:T(8,128)(2,1)} %reshape.119, s32[1024]{0:T(1024)S(1)} %pad_clamp_fusion.1), kind=kCustom, calls=%fused_computation.1 | custom fusion | bytes 2099200 | tf_op jit(solution)/shard_map/gather | solution.py:72
  442.2 2.4 reshape.120
  444.6 4.3 multiply_reduce_fusion
  448.9 0.1 multiply_reduce_fusion.1
  449.1 7.2 %all-gather.3 = f32[2,1,256]{2,1,0:T(1,128)S(1)} all-gather(f32[1,1,256]{2,1,0:T(1,128)S(1)} %bitcast.49), channel_id=3, replica_groups=mesh['grp'=2,'ep'=64,'tp'=2] {'tp'}, dimensions={0}, use_global_device_ids=true | all-gather | bytes 3072 | tf_op jit(solution)/shard_map/all_gather | solution.py:10
  456.2 1.0 multiply_convert_fusion
  (15 shorter events, 0.2 us)
Async XLA Ops:
  6.5 226.0 %copy-start = (bf16[1,512,2048]{2,1,0:T(8,128)(2,1)S(1)}, bf16[1,512,2048]{2,1,0:T(8,128)(2,1)}, u32[]{:S(2)}) copy-start(bf16[1,512,2048]{2,1,0:T(8,128)(2,1)} %param.12) | copy-start | bytes 6291460
  6.6 218.5 %all-gather.6.cloned.1.call-start = ((), (), s32[]{:S(2)}) async-start(), calls=%async_computation.3 | async-start | bytes 7864320 | tf_op jit(solution)/shard_map/all_gather | solution.py:56
  276.9 16.3 %copy-start.1 = (f32[256,2]{0,1:T(2,128)S(1)}, f32[256,2]{0,1:T(2,128)}, u32[]{:S(2)}) copy-start(f32[256,2]{0,1:T(2,128)} %param.14) | copy-start | bytes 6148
  276.9 16.5 %copy-start.2 = (bf16[1024]{0:T(1024)(128)(2,1)S(1)}, bf16[1024]{0:T(1024)(128)(2,1)}, u32[]{:S(2)}) copy-start(bf16[1024]{0:T(1024)(128)(2,1)} %param.15) | copy-start | bytes 6148
  276.9 155.4 %all-to-all-start.2 = ((bf16[64,20,1024]{2,1,0:T(8,128)(2,1)}), bf16[64,20,1024]{2,1,0:T(8,128)(2,1)}, u32[]{:S(2)}, u32[]{:S(2)}) async-start(bf16[64,20,1024]{2,1,0:T(8,128)(2,1)} %reshape_transpose_reshape.7), calls=%async_computation.2 | async-start | bytes 6291456 | tf_op jit(solution)/shard_map/all_to_all | solution.py:69
Sparse Core Ops, SparseCore 0:
  203.4 21.5 all-gather.5
where the time goes:
time: 465 us; the launch traced here: 464 us
  blocking collectives  188 us (40%)
  waiting for transfers between devices  161 us (35%)
  local copies, waits for them, and re-layouts  50.9 us (11%)
  matrix products  17.9 us (4%)
  other arithmetic  16.9 us (4%)
  starting transfers between devices  16.3 us (4%)
  between operations  13.6 us (3%)
    all_to_all x1, blocking collectives, body(): lax.all_to_all(outgoing, 'ep', split_axis=0, concat_axis=0, tiled=True)  150 us
    all_to_all x1, waiting for transfers between devices, body(): lax.all_to_all(homeward, 'ep', split_axis=0, concat_axis=0, tiled=True)  139 us
    all_gather x2, blocking collectives, total_of_pieces(): parts = lax.all_gather(x, axis)  29.1 us
    all_gather x1, waiting for transfers between devices, body(): piece = lax.all_gather(rows, 'tp', axis=2, tiled=True)  21.7 us
    all_to_all x1, starting transfers between devices, body(): lax.all_to_all(homeward, 'ep', split_axis=0, concat_axis=0, tiled=True)  16.3 us
    reshape x2, local copies, waits for them, and re-layouts, split_up(): x.reshape(*lengths[:dim], count, lengths[dim] // count, *lengths[dim + 1:])  13.6 us
    dot_general x1, matrix products, body(): jnp.einsum('erf,efd->erd', hidden, w_down, preferred_element_type=jnp.flo...  10.3 us
  transfers between devices with their start and end apart: 2, of which 2 were waited for; matrix products, arithmetic and copies ran while one was open for 0% of the time, Pallas kernels for 0%

commit v1 on v0

v1 whole, which is shorter than its diff:
```python
import functools

import jax
import jax.numpy as jnp
from jax import lax
from jax.experimental import pallas as pl
from jax.experimental.pallas import tpu as pltpu
from jax.sharding import PartitionSpec as P

GROUPS = 4
SHORT = 4
ROWS = 16
EPS = 1e-06
MESH = pl.DeviceIdType.MESH
F32 = jnp.float32
BF16 = jnp.bfloat16


def dot(a, b):
    return jnp.dot(a, b, preferred_element_type=F32)


def kernel(
    X, nz, slots,
    tok_ref, note_ref, first_gain, last_gain, gate_hbm, up_hbm, down_hbm,
    out_ref,
    blocks, notes, packs, rows, others, given, taken, done, back, mix, sums, total,
    before, sq_out, sq_in, gate_w, up_w, down_w,
    load_sem, ring_s, ring_r, note_s, note_r, pack_s, pack_r, half_s, half_r,
    part_s, part_r, back_s, back_r, sum_s, sum_r, sq_s, sq_r,
):
    T, half = tok_ref.shape
    C = T // 2
    H = nz // 2
    width = 2 * half
    ep = lax.axis_index("ep")
    tp = lax.axis_index("tp")
    z, x = ep // X, ep % X
    mate = 1 - tp
    ahead = lax.rem(z + 1 - 2 * tp + nz, nz) * X + x
    behind = lax.rem(z - 1 + 2 * tp + nz, nz) * X + x

    def peer(d):
        return lax.rem(x + d, X)

    barrier = pltpu.get_barrier_semaphore()
    for other in [ahead, behind] + [z * X + peer(d) for d in range(1, X)]:
        pl.semaphore_signal(barrier, inc=1, device_id={"ep": other}, device_id_type=MESH)
    pl.semaphore_signal(barrier, inc=1, device_id={"tp": mate}, device_id_type=MESH)

    loads = [
        pltpu.make_async_copy(gate_hbm.at[0], gate_w, load_sem.at[0]),
        pltpu.make_async_copy(up_hbm.at[0], up_w, load_sem.at[1]),
        pltpu.make_async_copy(down_hbm.at[0], down_w, load_sem.at[2]),
    ]
    for load in loads:
        load.start()

    def to_mate(src, dst, s, r):
        return pltpu.make_async_remote_copy(
            src_ref=src, dst_ref=dst, send_sem=s, recv_sem=r,
            device_id={"tp": mate}, device_id_type=MESH,
        )

    def to_ep(src, dst, s, r, other):
        return pltpu.make_async_remote_copy(
            src_ref=src, dst_ref=dst, send_sem=s, recv_sem=r,
            device_id={"ep": other}, device_id_type=MESH,
        )

    def sq_copy(n):
        return to_mate(sq_out.at[n], sq_in.at[n], sq_s.at[n], sq_r.at[n])

    def landing(way, k):
        return jnp.minimum(2 * k - 1 + tp, nz - 1) if way == 0 else 2 * k - tp

    def source(way, k):
        return jnp.where(k == 1, 0, landing(way, k - 1))

    def neighbour(way):
        return ahead if way == 0 else behind

    def ring(way, k, c):
        return to_ep(
            blocks.at[source(way, k), c], blocks.at[landing(way, k), c],
            ring_s.at[way, k - 1, c], ring_r.at[way, k - 1, c], neighbour(way),
        )

    def note(way, k):
        return to_ep(
            notes.at[source(way, k)], notes.at[landing(way, k)],
            note_s.at[way, k - 1], note_r.at[way, k - 1], neighbour(way),
        )

    def pack(b, d):
        return to_ep(
            packs.at[b, peer(d)], rows.at[b, x],
            pack_s.at[b, peer(d)], pack_r.at[b, x], z * X + peer(d),
        )

    def pack_in(b, d):
        return to_ep(
            packs.at[b, peer(d)], rows.at[b, peer(d)],
            pack_s.at[b, peer(d)], pack_r.at[b, peer(d)], z * X + peer(d),
        )

    def half_copy(b):
        return to_mate(rows.at[b], others.at[b], half_s.at[b], half_r.at[b])

    def part_copy(b):
        return to_mate(given.at[b], taken.at[b], part_s.at[b], part_r.at[b])

    def home(b, d):
        return to_ep(
            done.at[b, peer(d)], back.at[b, x],
            back_s.at[b, peer(d)], back_r.at[b, x], z * X + peer(d),
        )

    def home_in(b, d):
        return to_ep(
            done.at[b, peer(d)], back.at[b, peer(d)],
            back_s.at[b, peer(d)], back_r.at[b, peer(d)], z * X + peer(d),
        )

    def sum_copy(way, k, c):
        return to_ep(
            blocks.at[landing(way, k), c], sums.at[way, k - 1, c],
            sum_s.at[way, k - 1, c], sum_r.at[way, k - 1, c], neighbour(1 - way),
        )

    narrow = tok_ref[...].astype(F32)
    own = jnp.broadcast_to(jnp.sum(narrow * narrow, axis=1, keepdims=True), (T, 128))
    sq_out[0] = own
    notes[0] = note_ref[...]
    below = lax.broadcasted_iota(jnp.int32, (T, T), 0) < lax.broadcasted_iota(jnp.int32, (T, T), 1)
    before[...] = below.astype(F32).astype(BF16)
    pl.semaphore_wait(barrier, X + 2)
    sq_copy(0).start()
    sq_copy(0).wait_recv()
    scale = lax.rsqrt((sq_out[0] + sq_in[0])[:, :1] / width + EPS)
    normed = tok_ref[...].astype(F32) * scale * first_gain[...].astype(F32)
    blocks[0] = normed.astype(BF16).reshape(2, C, half)

    def step(i, carry):
        k, c = i // 2, i % 2
        for way in range(2):
            last = H - way

            @pl.when((k >= 1) & (k <= last))
            def _():
                @pl.when(c == 0)
                def _():
                    note(way, k).wait_recv()

                ring(way, k, c).wait_recv()

            @pl.when(k < last)
            def _():
                @pl.when(c == 0)
                def _():
                    note(way, k + 1).start()

                ring(way, k + 1, c).start()

        @pl.when((i >= 2) & (i < nz + 2))
        def _():
            b = i - 2
            tag = notes[b]
            ids = (lax.broadcasted_iota(jnp.int32, (8, T), 0) + z * X).astype(F32)
            first, second = tag[0:1] == ids, tag[1:2] == ids
            hit = first | second
            rank = dot(hit.astype(F32).astype(BF16), before[...])
            key = jnp.where(hit, rank, -1.0)
            weight = jnp.where(first, tag[2:3], 0.0) + jnp.where(second, tag[3:4], 0.0)
            place = lax.broadcasted_iota(jnp.int32, (slots, T), 0).astype(F32)
            chosen, scaled = [], []
            for e in range(X):
                mark = key[e : e + 1] == place
                chosen.append(mark.astype(F32).astype(BF16))
                scaled.append(jnp.where(mark, weight[e : e + 1], 0.0))
            pick = jnp.concatenate(chosen, axis=0)
            spread = jnp.concatenate(scaled, axis=0).T
            high = spread.astype(BF16)
            low = (spread - high.astype(F32)).astype(BF16)
            mix[b] = jnp.concatenate([high, low], axis=1).reshape(2, C, 2 * X * slots)
            packs[b] = dot(pick, blocks[b].reshape(T, half)).astype(BF16).reshape(X, slots, half)
            rows[b, x] = packs[b, x]
            for d in range(1, X):
                pack(b, d).start()

        @pl.when((i >= 3) & (i < nz + 3))
        def _():
            b = i - 3
            for d in range(1, X):
                pack_in(b, d).wait_recv()
            half_copy(b).start()

        @pl.when(i == 4)
        def _():
            for load in loads:
                load.wait()

        @pl.when((i >= 4) & (i < nz + 4))
        def _():
            b = i - 4
            half_copy(b).wait_recv()
            mine = rows[b].reshape(X * slots, half)
            other = others[b].reshape(X * slots, half)
            near = pl.ds(pl.multiple_of(tp * half, half), half)
            far = pl.ds(pl.multiple_of(mate * half, half), half)
            gate = dot(mine, gate_w[near, :]) + dot(other, gate_w[far, :])
            upper = dot(mine, up_w[near, :]) + dot(other, up_w[far, :])
            hidden = (gate / (1.0 + jnp.exp(-gate)) * upper).astype(BF16)
            given[b] = dot(hidden, down_w[:, far]).astype(BF16).reshape(X, slots, half)
            part_copy(b).start()
            done[b] = dot(hidden, down_w[:, near]).astype(BF16).reshape(X, slots, half)

        @pl.when(i >= 5)
        def _():
            b = i - 5
            part_copy(b).wait_recv()
            done[b] = (done[b].astype(F32) + taken[b].astype(F32)).astype(BF16)
            for d in range(1, X):
                home(b, d).start()
            back[b, x] = done[b, x]

        return carry

    lax.fori_loop(0, nz + 5, step, 0)

    def drain(n, carry):
        for way in range(2):

            @pl.when(n < H - way)
            def _():
                note(way, n + 1).wait_send()
                for c in range(2):
                    ring(way, n + 1, c).wait_send()

        for d in range(1, X):
            pack(n, d).wait_send()
        half_copy(n).wait_send()
        part_copy(n).wait_send()
        return carry

    lax.fori_loop(0, nz, drain, 0)

    def arrive(b):
        for d in range(1, X):
            home_in(b, d).wait_recv()

    def share(b, c):
        made = back[b].reshape(X * slots, half)
        return dot(mix[b, c], jnp.concatenate([made, made], axis=0))

    def unwind(i, carry):
        j, c = i // 2, i % 2
        for way in range(2):
            last = H - way
            k = last - j
            b = landing(way, k)

            @pl.when((k >= 1) & (c == 0))
            def _():
                arrive(b)

            @pl.when(k == last)
            def _():
                blocks[b, c] = share(b, c).astype(BF16)
                sum_copy(way, k, c).start()

            @pl.when((k >= 1) & (k < last))
            def _():
                part = share(b, c)
                sum_copy(way, k + 1, c).wait_recv()
                blocks[b, c] = (part + sums[way, k, c].astype(F32)).astype(BF16)
                sum_copy(way, k, c).start()

        return carry

    lax.fori_loop(0, 2 * H, unwind, 0)

    arrive(0)
    for c in range(2):
        part = share(0, c)
        for way in range(2):
            sum_copy(way, 1, c).wait_recv()
        mixed = part + sums[0, 0, c].astype(F32) + sums[1, 0, c].astype(F32)
        total[c] = mixed
        sq_out[1, pl.ds(c * C, C), :] = jnp.broadcast_to(
            jnp.sum(mixed * mixed, axis=1, keepdims=True), (C, 128)
        )
    sq_copy(1).start()
    sq_copy(1).wait_recv()
    norm = lax.rsqrt((sq_out[1] + sq_in[1])[:, :1] / width + EPS)
    out_ref[...] = (total[...].reshape(T, half) * norm * last_gain[...].astype(F32)).astype(BF16)

    for n in range(2):
        sq_copy(n).wait_send()

    def finish(n, carry):
        for d in range(1, X):
            home(n, d).wait_send()
        for way in range(2):

            @pl.when(n < H - way)
            def _():
                for c in range(2):
                    sum_copy(way, n + 1, c).wait_send()

        return carry

    lax.fori_loop(0, nz, finish, 0)


def body(tokens, norm_gain, w_gate, w_up, w_down, expert_ids, combine, final_gain, X=SHORT):
    T, half = tokens.shape
    n_ep = lax.axis_size("ep")
    nz = n_ep // X
    H = nz // 2
    per_group = n_ep * w_gate.shape[0] // GROUPS
    capacity = T // 8 * 5 * 2 // per_group
    slots = -(-capacity // ROWS) * ROWS
    hidden = w_gate.shape[2]
    C = T // 2
    note = jnp.concatenate(
        [expert_ids.T.astype(F32), combine.T, jnp.zeros((4, T), F32)], axis=0
    )
    piece = (nz, X, slots, half)
    vmem = pl.BlockSpec(memory_space=pltpu.VMEM)
    hbm = pl.BlockSpec(memory_space=pl.ANY)
    dma = pltpu.SemaphoreType.DMA
    return pl.pallas_call(
        functools.partial(kernel, X, nz, slots),
        out_shape=jax.ShapeDtypeStruct((T, half), BF16),
        in_specs=[vmem] * 4 + [hbm] * 3,
        out_specs=vmem,
        scratch_shapes=[
            pltpu.VMEM((nz, 2, C, half), BF16),
            pltpu.VMEM((nz, 8, T), F32),
            pltpu.VMEM(piece, BF16),
            pltpu.VMEM(piece, BF16),
            pltpu.VMEM(piece, BF16),
            pltpu.VMEM(piece, BF16),
            pltpu.VMEM(piece, BF16),
            pltpu.VMEM(piece, BF16),
            pltpu.VMEM(piece, BF16),
            pltpu.VMEM((nz, 2, C, 2 * X * slots), BF16),
            pltpu.VMEM((2, H, 2, C, half), BF16),
            pltpu.VMEM((2, C, half), F32),
            pltpu.VMEM((T, T), BF16),
            pltpu.VMEM((2, T, 128), F32),
            pltpu.VMEM((2, T, 128), F32),
            pltpu.VMEM((2 * half, hidden), BF16),
            pltpu.VMEM((2 * half, hidden), BF16),
            pltpu.VMEM((hidden, 2 * half), BF16),
            dma((3,)),
            dma((2, H, 2)),
            dma((2, H, 2)),
            dma((2, H)),
            dma((2, H)),
            dma((nz, X)),
            dma((nz, X)),
            dma((nz,)),
            dma((nz,)),
            dma((nz,)),
            dma((nz,)),
            dma((nz, X)),
            dma((nz, X)),
            dma((2, H, 2)),
            dma((2, H, 2)),
            dma((2,)),
            dma((2,)),
        ],
        compiler_params=pltpu.CompilerParams(
            collective_id=0, has_side_effects=True, vmem_limit_bytes=62 * 1024 * 1024
        ),
    )(tokens, note, norm_gain.reshape(1, half), final_gain.reshape(1, half), w_gate, w_up, w_down)


def solution(mesh):
    placed = (
        P(("grp", "ep"), "tp"),
        P("tp"),
        P("ep", None, "tp"),
        P("ep", None, "tp"),
        P("ep", "tp", None),
        P(("grp", "ep"), None),
        P(("grp", "ep"), None),
        P("tp"),
    )
    return jax.shard_map(
        body, mesh=mesh, in_specs=placed, out_specs=P(("grp", "ep"), "tp"), check_vma=False
    )
```

time: 465 us -> 239 us (0.51)
  Pallas kernels: 0 us -> 232 us
  blocking collectives: 188 us -> 0 us
  waiting for transfers between devices: 161 us -> 0 us
  local copies, waits for them, and re-layouts: 50.9 us -> 4.49 us
  matrix products: 17.9 us -> 0 us
  starting transfers between devices: 16.3 us -> 0 us
  other arithmetic: 16.9 us -> 2.03 us
  between operations: 13.6 us -> 0.01 us
    pallas_call x0 -> x1, Pallas kernels: none -> 232 us  [body(): pl.pallas_call(functools.partial(kernel, X, nz, slots), out_shape=jax.Sha...]
    all_to_all x2 -> x0, blocking collectives: 159 us -> none  [the longest x1 150 us: body(): lax.all_to_all(outgoing, 'ep', split_axis=0, concat_axis=0, tiled=True)]
    all_to_all x1 -> x0, waiting for transfers between devices: 139 us -> none  [body(): lax.all_to_all(homeward, 'ep', split_axis=0, concat_axis=0, tiled=True)]
    all_gather x2 -> x0, blocking collectives: 29.1 us -> none  [total_of_pieces(): parts = lax.all_gather(x, axis)]
    all_gather x1 -> x0, waiting for transfers between devices: 21.7 us -> none  [body(): piece = lax.all_gather(rows, 'tp', axis=2, tiled=True)]
    reshape x4 -> x2, local copies, waits for them, and re-layouts: 23.9 us -> 2.54 us  [the longest x1 1.28 us: body(): norm_gain.reshape(1, half)]
    dot_general x2 -> x0, matrix products: 17.9 us -> none  [the longest x1 10.3 us: body(): jnp.einsum('erf,efd->erd', hidden, w_down, preferred_element_type=jnp.flo...]
    all_to_all x1 -> x0, starting transfers between devices: 16.3 us -> none  [body(): lax.all_to_all(homeward, 'ep', split_axis=0, concat_axis=0, tiled=True)]
  transfers between devices with their start and end apart: 2 -> 0, of which waited for: 2 -> 0; matrix products, arithmetic and copies ran while one was open for 0% -> 0% of each run, Pallas kernels for 0% -> 0%
where the time goes in v1:
time: 239 us; the launch traced here: 238 us
  Pallas kernels  232 us (97%)
  local copies, waits for them, and re-layouts  4.49 us (2%)
    pallas_call x1, Pallas kernels, body(): pl.pallas_call(functools.partial(kernel, X, nz, slots), out_shape=jax.Sha...  232 us

profile of v1, /device:TPU:33, one launch (start us, length us, event | category | flops | bytes accessed | tf_op | source)
XLA Modules:
  0.0 238.4 jit_solution(11549053753103678768)
XLA Ops:
  0.0 0.1 pad.2.clone
  0.1 0.7 convert_bitcast_fusion
  0.8 1.3 reshape.6.first_gain
  2.0 1.3 reshape.7.last_gain
  3.3 1.3 maximum_maximum_fusion.note_ref
  4.7 231.8 %shard_map.82 = bf16[256,1024]{1,0:T(8,128)(2,1)} custom-call(bf16[256,1024]{1,0:T(8,128)(2,1)} %tok_ref.1, f32[8,256]{1,0:T(8,128)} %maximum_maximum_fusion.note_ref, bf16[1,1024]{1,0:T(2,128)(2,1)} %reshape.6.first_gain, bf16[1,1024]{1,0:T(2,128)(2,1)} %reshape.7.last_gain, bf16[1,2048,512]{2,1,0:T(8,128)(2,1)} %gate_hbm.1, bf16[1,2048,512]{2,1,0:T(8,128)(2,1)} %up_hbm.1, ...), custom_call_target="tpu_custom_call" | custom-call | tf_op jit(solution)/shard_map/pallas_call | solution.py:333
  236.5 1.9 copy.10
  (1 shorter events, 0.0 us)
